TPU v7x, 32 devices: a whole 2x2x4 slice. The times are simulated.
32 devices in a mesh: ep: 8 (over z, y), tp: 4 (over x, core).
Axes of the slice: x: 2, y: 2, z: 4, core: 2. Of those that a mesh axis runs over, the one named last changes fastest.
Arguments:
- mixer_input: bfloat16 [4096, 2048], P('ep'), may hold values from -6 to 6
- log_forget_total: float32 [16, 4096], P('tp'), may hold values from -684 to 0, as said below
- mixer_gain: float32 [2048], replicated, may hold values from 0.1 to 1.9
- w_query: bfloat16 [2048, 1024], P(None, 'tp'), may hold values from -1 to 1
- w_key: bfloat16 [2048, 256], P(None, 'tp'), may hold values from -8 to 8
- w_value: bfloat16 [2048, 256], P(None, 'tp'), may hold values from -0.125 to 0.125
- w_output: bfloat16 [1024, 2048], replicated, may hold values from -0.1875 to 0.1875
- mixer_post_gain: float32 [2048], replicated, may hold values from 0.1 to 1.9
- expert_input: bfloat16 [2048, 2048], P('ep'), may hold values from -6 to 6
- expert_ids: int32 [2048, 2], P('ep'), may hold values from 0 to 7, all different within a row; in each aligned block of 64 rows (0 to 63, 64 to 127, ...) at most 32 rows name the same one
- route_weight: float32 [2048, 2], P('ep'), may hold values from 0.1 to 1
- expert_gain: float32 [2048], replicated, may hold values from 0.1 to 1.9
- w_gate: bfloat16 [8, 2048, 3584], P('ep', None, 'tp'), may hold values from -0.125 to 0.125
- w_up: bfloat16 [8, 2048, 3584], P('ep', None, 'tp'), may hold values from -0.125 to 0.125
- w_down: bfloat16 [8, 3584, 2048], P('ep', 'tp'), may hold values from -0.09375 to 0.09375
- expert_post_gain: float32 [2048], replicated, may hold values from 0.1 to 1.9
Outputs:
- mixer_out: bfloat16 [4096, 2048], P(('ep', 'tp'))
- expert_out: bfloat16 [2048, 2048], P(('ep', 'tp'))
Inputs may be any that keep to these rules, and one draw needn't show every extreme that they name: `expert_ids`: in each aligned block of 64 tokens no expert is named by more than 32 of them. `log_forget_total`: each head's values never rise along the positions.
All inputs are finite; a program needn't handle non-finite values.
Results may differ from a plain program's by a relative error of at most 0.012.
The roundings to bfloat16 on the way count: a program that leaves them out, or rounds other values in their place, can miss the bound.
Values may be sent and summed in bfloat16 or wider, within the bound.
A program may use at most 128 MiB of HBM per device.

v0:
```python
import math

import jax
import jax.numpy as jnp
from jax import lax
from jax.sharding import PartitionSpec as P

HD = 64
TOP_K = 2


NEG_FILL = -1e30
NORM_EPS = 1e-06


def norm_rows(values_in, gain_vec):
    widened = values_in.astype(jnp.float32)
    return (
        widened
        * lax.rsqrt(jnp.mean(widened * widened, axis=-1, keepdims=True) + NORM_EPS)
        * gain_vec
    )


def unchanged(present_state):
    return present_state


def mixer_half(
    mixer_input, log_forget_total, mixer_gain, w_query, w_key, w_value, w_output, mixer_post_gain
):
    row_count = mixer_input.shape[0]
    offset = lax.axis_index("ep") * row_count
    head_local = w_query.shape[1] // HD
    kv_local = w_key.shape[1] // HD
    group_size = head_local // kv_local
    normed = norm_rows(mixer_input, mixer_gain).astype(jnp.bfloat16)
    queries = (
        jnp.dot(normed, w_query, preferred_element_type=jnp.float32)
        .astype(jnp.bfloat16)
        .reshape(row_count, kv_local, group_size, HD)
    )
    key_rows = (
        jnp.dot(normed, w_key, preferred_element_type=jnp.float32)
        .astype(jnp.bfloat16)
        .reshape(row_count, kv_local, HD)
    )
    value_rows = (
        jnp.dot(normed, w_value, preferred_element_type=jnp.float32)
        .astype(jnp.bfloat16)
        .reshape(row_count, kv_local, HD)
    )
    gate_totals = log_forget_total.reshape(kv_local, group_size, -1)
    query_gate = lax.dynamic_slice_in_dim(gate_totals, offset, row_count, 2)
    query_pos = offset + jnp.arange(row_count, dtype=jnp.int32)
    last_row = offset + row_count - 1
    score_scale = HD ** (-0.5)
    start_state = (
        jnp.full((kv_local, group_size, row_count), NEG_FILL, jnp.float32),
        jnp.zeros((kv_local, group_size, row_count), jnp.float32),
        jnp.zeros((kv_local, group_size, row_count, HD), jnp.float32),
    )
    running = start_state
    key_piece = lax.all_gather(key_rows, "ep", axis=0, tiled=True)
    value_piece = lax.all_gather(value_rows, "ep", axis=0, tiled=True)
    piece_rows = key_piece.shape[0]
    block_rows = math.gcd(piece_rows, 512)
    block_total = piece_rows // block_rows
    key_blocks = key_piece.reshape(block_total, block_rows, kv_local, HD)
    value_blocks = value_piece.reshape(block_total, block_rows, kv_local, HD)

    def one_block(present_state, operands):
        key_block, value_block, block_index = operands
        block_first = block_index * block_rows

        def update(prior_value):
            row_max, denominator, numerator = prior_value
            key_gate = lax.dynamic_slice_in_dim(gate_totals, block_first, block_rows, 2)
            scores = (
                jnp.einsum("qgjd,kgd->gjqk", queries, key_block, preferred_element_type=jnp.float32)
                * score_scale
            )
            scores = scores + query_gate[:, :, :, None] - key_gate[:, :, None, :]
            visible = (block_first + jnp.arange(block_rows, dtype=jnp.int32))[None, :] <= query_pos[
                :, None
            ]
            scores = jnp.where(visible, scores, NEG_FILL)
            new_max = jnp.maximum(row_max, jnp.max(scores, axis=-1))
            shifted = jnp.where(visible, jnp.exp(scores - new_max[..., None]), 0.0)
            factor = jnp.exp(row_max - new_max)
            denominator = denominator * factor + jnp.sum(shifted, axis=-1)
            numerator = numerator * factor[..., None] + jnp.einsum(
                "gjqk,kgd->gjqd",
                shifted.astype(jnp.bfloat16),
                value_block,
                preferred_element_type=jnp.float32,
            )
            return (new_max, denominator, numerator)

        return (lax.cond(block_first <= last_row, update, unchanged, present_state), None)

    running, _ = lax.scan(
        one_block, running, (key_blocks, value_blocks, jnp.arange(block_total, dtype=jnp.int32))
    )
    row_max, denominator, numerator = running
    mixed_heads = (
        jnp.transpose(numerator / denominator[..., None], (2, 0, 1, 3))
        .reshape(row_count, head_local * HD)
        .astype(jnp.bfloat16)
    )
    by_rows = lax.all_to_all(mixed_heads, "tp", split_axis=0, concat_axis=1, tiled=True)
    projected = jnp.dot(by_rows, w_output, preferred_element_type=jnp.float32)
    return norm_rows(projected, mixer_post_gain).astype(jnp.bfloat16)


def expert_half(
    expert_input, expert_ids, route_weight, expert_gain, w_gate, w_up, w_down, expert_post_gain
):
    row_count = expert_input.shape[0]
    quarters = lax.axis_size("tp")
    experts = lax.axis_size("ep")
    quarter_rows = row_count // quarters
    slot_count = 2 * TOP_K * quarter_rows // experts
    own_quarter = lax.axis_index("tp")
    normed = norm_rows(expert_input, expert_gain).astype(jnp.bfloat16)
    padded_rows = jnp.concatenate([normed, jnp.zeros((1, normed.shape[1]), jnp.bfloat16)], axis=0)
    routed = expert_ids.reshape(quarters, quarter_rows * TOP_K)
    matches = (routed[:, :, None] == jnp.arange(experts, dtype=jnp.int32)[None, None, :]).astype(
        jnp.int32
    )
    slot_ranks = jnp.sum(jnp.cumsum(matches, axis=1) * matches, axis=2) - 1
    owners = (jnp.arange(row_count * TOP_K, dtype=jnp.int32) // TOP_K).reshape(
        quarters, quarter_rows * TOP_K
    )
    quarter_index = jnp.broadcast_to(jnp.arange(quarters, dtype=jnp.int32)[:, None], routed.shape)
    slot_table = (
        jnp.full((quarters, slot_count, experts), row_count, jnp.int32)
        .at[quarter_index, slot_ranks, routed]
        .set(owners)
    )
    gate_local = w_gate[0]
    up_local = w_up[0]
    down_local = w_down[0]
    unit_count = gate_local.shape[1]
    own_table = lax.dynamic_index_in_dim(slot_table, own_quarter, 0, keepdims=False)
    outgoing = padded_rows[own_table]
    arrived = lax.all_to_all(outgoing, "ep", split_axis=1, concat_axis=1, tiled=True)
    slot_rows = lax.all_gather(arrived[None], "tp", axis=0, tiled=True)
    flat_rows = slot_rows.reshape(-1, slot_rows.shape[-1])
    gate_part = jnp.dot(flat_rows, gate_local, preferred_element_type=jnp.float32)
    up_part = jnp.dot(flat_rows, up_local, preferred_element_type=jnp.float32)
    hidden = (
        (jax.nn.silu(gate_part) * up_part)
        .astype(jnp.bfloat16)
        .reshape(slot_rows.shape[:-1] + (unit_count,))
    )
    product = jnp.dot(
        hidden.reshape(-1, unit_count), down_local, preferred_element_type=jnp.float32
    )
    summed = lax.psum_scatter(
        product.reshape(lax.axis_size("tp") * 1, slot_count, experts, product.shape[-1]).astype(
            jnp.bfloat16
        ),
        "tp",
        scatter_dimension=0,
        tiled=True,
    ).astype(jnp.float32)
    results = summed[0].astype(jnp.bfloat16)
    returned = lax.all_to_all(results, "ep", split_axis=1, concat_axis=1, tiled=True)
    flat_results = returned.reshape(slot_count * experts, returned.shape[-1])
    own_routes = lax.dynamic_index_in_dim(routed, own_quarter, 0, keepdims=False)
    own_ranks = lax.dynamic_index_in_dim(slot_ranks, own_quarter, 0, keepdims=False)
    picked = flat_results[own_ranks * experts + own_routes].reshape(quarter_rows, TOP_K, -1)
    own_weights = lax.dynamic_slice_in_dim(
        route_weight, own_quarter * quarter_rows, quarter_rows, 0
    )
    combined = jnp.sum(own_weights[:, :, None] * picked.astype(jnp.float32), axis=1)
    return norm_rows(combined, expert_post_gain).astype(jnp.bfloat16)


def per_device(
    mixer_input,
    log_forget_total,
    mixer_gain,
    w_query,
    w_key,
    w_value,
    w_output,
    mixer_post_gain,
    expert_input,
    expert_ids,
    route_weight,
    expert_gain,
    w_gate,
    w_up,
    w_down,
    expert_post_gain,
):
    mixer_out = mixer_half(
        mixer_input,
        log_forget_total,
        mixer_gain,
        w_query,
        w_key,
        w_value,
        w_output,
        mixer_post_gain,
    )
    expert_out = expert_half(
        expert_input, expert_ids, route_weight, expert_gain, w_gate, w_up, w_down, expert_post_gain
    )
    return (mixer_out, expert_out)


def solution(mesh):
    placed = (
        P("ep", None),
        P("tp", None),
        P(),
        P(None, "tp"),
        P(None, "tp"),
        P(None, "tp"),
        P(),
        P(),
        P("ep", None),
        P("ep", None),
        P("ep", None),
        P(),
        P("ep", None, "tp"),
        P("ep", None, "tp"),
        P("ep", "tp", None),
        P(),
    )
    return jax.shard_map(
        per_device,
        mesh=mesh,
        in_specs=placed,
        out_specs=(P(("ep", "tp"), None), P(("ep", "tp"), None)),
        check_vma=False,
    )
```

profile of v0, /device:TPU:0, one launch (start us, length us, event | category | flops | bytes accessed | tf_op | source)
XLA Modules:
  0.0 324.2 jit_solution(3863174267052389493)
XLA Ops:
  7.2 0.9 copy.41
  9.2 29.5 %scatter_fusion = s32[4,32,8]{1,2,0:T(8,128)S(1)} fusion(s32[4,32,8]{1,2,0:T(8,128)S(1)} %broadcast_in_dim.39, s32[512]{0:T(512)S(1)} %fusion.52, s32[512]{0:T(512)S(1)} %fusion.54), kind=kCustom, calls=%fused_computation.2 | custom fusion | bytes 12288 | tf_op jit(solution)/shard_map/scatter | solution.py:139
  39.7 1.4 gather_fusion
  41.0 0.6 copy.44
  41.6 32.9 %all_to_all.26 = bf16[32,8,2048]{2,0,1:T(8,128)(2,1)S(1)} all-to-all(bf16[32,8,2048]{2,0,1:T(8,128)(2,1)S(1)} %copy.44), channel_id=1, replica_groups=mesh['ep'=8,'tp'=4] {'ep'}, dimensions={1} | all-to-all | bytes 2097152 | tf_op jit(solution)/shard_map/all_to_all | solution.py:147
  74.5 1.6 copy.45
  76.3 33.4 %all-gather.5.cloned.1.call-done = bf16[128,8,2048]{2,1,0:T(8,128)(2,1)} async-done(((bf16[32,8,2048]{2,1,0:T(8,128)(2,1)}), bf16[128,8,2048]{2,1,0:T(8,128)(2,1)}) %all-gather.5.cloned.1.call-update) | async-done | bytes 4194320 | tf_op jit(solution)/shard_map/all_gather | solution.py:148
  109.7 7.5 %fusion.32 = f32[1024,896]{1,0:T(8,128)S(1)} fusion(bf16[128,8,2048]{2,1,0:T(8,128)(2,1)} %all-gather.5.cloned.1.call-done, bf16[1,2048,896]{2,1,0:T(8,128)(2,1)} %param.33), kind=kOutput, calls=%fused_computation.40 | convolution fusion | flops 3758096384 | bytes 11534336 | tf_op jit(solution)/shard_map/dot_general | solution.py:151
  117.2 4.8 %multiply_convert_fusion = bf16[1024,896]{1,0:T(8,128)(2,1)S(1)} fusion(f32[1024,896]{1,0:T(8,128)S(1)} %fusion.32, bf16[1,2048,896]{2,1,0:T(8,128)(2,1)S(1)} %copy-done.11, bf16[128,8,2048]{2,1,0:T(8,128)(2,1)S(1)} %copy-done.10), kind=kOutput, calls=%fused_computation.48 | convolution fusion | flops 3763601408 | bytes 13369344 | tf_op jit(solution)/shard_map/dot_general | solution.py:150
  122.0 6.0 %convolution_convert_fusion = bf16[4,32,8,2048]{3,2,1,0:T(8,128)(2,1)} fusion(bf16[4,32,8,896]{3,2,1,0:T(8,128)(2,1)S(1)} %bitcast.163, bf16[1,896,2048]{2,1,0:T(8,128)(2,1)S(1)} %copy-done.12), kind=kOutput, calls=%fused_computation.44 | convolution fusion | flops 3760193536 | bytes 9699328 | tf_op jit(solution)/shard_map/dot_general | solution.py:157
  128.0 1.5 copy-done.1
  129.6 0.5 fusion.29
  130.1 2.2 fusion.31
  132.3 0.8 convolution_convert_fusion.3
  133.0 31.5 %all-gather = bf16[4096,64]{0,1:T(8,128)(2,1)S(1)} all-gather(bf16[512,64]{0,1:T(8,128)(2,1)S(1)} %convolution_convert_fusion.3), channel_id=2, replica_groups=mesh['ep'=8,'tp'=4] {'ep'}, dimensions={0}, use_global_device_ids=true | all-gather | bytes 589824 | tf_op jit(solution)/shard_map/all_gather | solution.py:64
  164.7 0.9 copy.37
  165.6 0.8 convolution_convert_fusion.2
  166.4 31.4 %all-gather.1 = bf16[4096,64]{0,1:T(8,128)(2,1)S(1)} all-gather(bf16[512,64]{0,1:T(8,128)(2,1)S(1)} %convolution_convert_fusion.2), channel_id=3, replica_groups=mesh['ep'=8,'tp'=4] {'ep'}, dimensions={0}, use_global_device_ids=true | all-gather | bytes 589824 | tf_op jit(solution)/shard_map/all_gather | solution.py:65
  198.0 1.0 copy.38
  199.0 0.7 dynamic-slice_bitcast_fusion.1
  199.7 1.5 convolution_convert_fusion.1
  201.2 18.1 %while.15 = (s32[]{:T(128)}, f32[1,4,512]{2,1,0:T(4,128)S(1)}, f32[1,4,512]{2,1,0:T(4,128)S(1)}, f32[1,4,512,64]{2,3,1,0:T(8,128)S(1)}, s32[8]{0:T(128)S(1)}, /*...) while((s32[]{:T(128)}, f32[1,4,512]{2,1,0:T(4,128)S(1)}, ...), condition=%wide.region_6.7_spmd.clone, body=%wide.region_1.6_spmd.clone.sunk | while | flops 288889856 | bytes 15283569 | solution.py:102
  201.2 0.7 dynamic_slice.79
  202.5 7.4 %conditional.3 = ((f32[1,4,512]{2,1,0:T(4,128)S(1)}, f32[1,4,512]{2,1,0:T(4,128)S(1)}, f32[1,4,512,64]{2,3,1,0:T(8,128)S(1)})) conditional(s32[]{:T(128)} %convert_element_type.123, (f32[1,4,512]{2,1,0:T(4,128)S(1)}, f32[1,4,512]{2,1,0:T(4,128)S(1)}, f32[1,4,512,64]{2,3,1,0:T(8,128)S(1)}) %tuple.48, (s32[]{:T(128)}, s32[]{:T(128)}, ...), branch_computations={%region_2.2_spmd, %region_3.5_spmd} | conditional | flops 288889856 | bytes 15281230 | solution.py:100
  202.5 0.8 dynamic-slice_bitcast_fusion
  203.6 2.2 fusion.6
  205.8 2.6 fusion.14
  208.4 1.5 fusion.5
  210.0 0.7 dynamic_slice.79
  211.3 0.7 dynamic_slice.79
  212.6 0.7 dynamic_slice.79
  214.0 0.7 dynamic_slice.79
  215.3 0.7 dynamic_slice.79
  216.7 0.7 dynamic_slice.79
  218.0 0.7 dynamic_slice.79
  219.5 0.7 copy.39
  220.2 3.4 %all-to-all-start = ((bf16[4,128,256]{1,2,0:T(8,128)(2,1)}), bf16[4,128,256]{1,2,0:T(8,128)(2,1)S(1)}, u32[]{:S(2)}, u32[]{:S(2)}) async-start(bf16[4,128,256]{1,2,0:T(8,128)(2,1)} %copy.39), calls=%async_computation | async-start | bytes 524288 | tf_op jit(solution)/shard_map/all_to_all | solution.py:111
  223.7 2.8 copy.46
  226.5 3.1 all-to-all-done
  229.6 57.5 %all-to-all-start.2 = ((bf16[32,8,2048]{2,0,1:T(8,128)(2,1)}), bf16[32,8,2048]{2,0,1:T(8,128)(2,1)S(1)}, u32[]{:S(2)}, u32[]{:S(2)}) async-start(bf16[32,8,2048]{2,0,1:T(8,128)(2,1)} %copy.46), calls=%async_computation.3 | async-start | bytes 2097152 | tf_op jit(solution)/shard_map/all_to_all | solution.py:169
  287.3 3.0 multiply_reduce_fusion.1
  290.3 1.0 multiply_convert_fusion.1
  291.3 21.4 %all-to-all-done.2 = bf16[32,8,2048]{2,0,1:T(8,128)(2,1)S(1)} async-done(((bf16[32,8,2048]{2,0,1:T(8,128)(2,1)}), bf16[32,8,2048]{2,0,1:T(8,128)(2,1)S(1)}, u32[]{:S(2)}, u32[]{:S(2)}) %all-to-all-start.2) | async-done | bytes 1048608 | tf_op jit(solution)/shard_map/all_to_all | solution.py:169
  312.7 0.6 copy.53
  313.3 0.9 gather_fusion.1
  314.2 0.7 reshape.287
  314.9 1.5 multiply_reduce_fusion
  316.6 0.8 multiply_convert_fusion.2
  (83 shorter events, 3.4 us)
Async XLA Ops:
  7.2 192.5 %copy-start = (bf16[2048,256]{1,0:T(8,128)(2,1)S(1)}, bf16[2048,256]{1,0:T(8,128)(2,1)}, u32[]{:S(2)}) copy-start(bf16[2048,256]{1,0:T(8,128)(2,1)} %param.23) | copy-start | bytes 3145732
  7.2 31.8 %copy-start.2 = (bf16[256,2048]{1,0:T(8,128)(2,1)S(1)}, bf16[256,2048]{1,0:T(8,128)(2,1)}, u32[]{:S(2)}) copy-start(bf16[256,2048]{1,0:T(8,128)(2,1)} %param.28) | copy-start | bytes 3145732
  7.2 32.1 %copy-start.5 = (f32[2048]{0:T(1024)S(1)}, f32[2048]{0:T(1024)}, u32[]{:S(2)}) copy-start(f32[2048]{0:T(1024)} %param.31) | copy-start | bytes 24580
  7.2 102.5 %all-gather.5.cloned.1.call-start = ((), (), s32[]{:S(2)}) async-start(), calls=%async_computation.5 | async-start | bytes 5242880 | tf_op jit(solution)/shard_map/all_gather | solution.py:148
  76.1 147.6 %reduce-scatter.2.cloned.1.call-start = ((), (), s32[]{:S(2)}) async-start(), calls=%async_computation.4 | async-start | bytes 5242880 | tf_op jit(solution)/shard_map/reduce_scatter | solution.py:160
  109.7 7.5 %copy-start.10 = (bf16[128,8,2048]{2,1,0:T(8,128)(2,1)S(1)}, bf16[128,8,2048]{2,1,0:T(8,128)(2,1)}, u32[]{:S(2)}) copy-start(bf16[128,8,2048]{2,1,0:T(8,128)(2,1)} %all-gather.5.cloned.1.call-done) | copy-start | bytes 12582916
  109.7 7.5 %copy-start.11 = (bf16[1,2048,896]{2,1,0:T(8,128)(2,1)S(1)}, bf16[1,2048,896]{2,1,0:T(8,128)(2,1)}, u32[]{:S(2)}) copy-start(bf16[1,2048,896]{2,1,0:T(8,128)(2,1)} %param.32) | copy-start | bytes 11010052
  117.2 4.8 %copy-start.12 = (bf16[1,896,2048]{2,1,0:T(8,128)(2,1)S(1)}, bf16[1,896,2048]{2,1,0:T(8,128)(2,1)}, u32[]{:S(2)}) copy-start(bf16[1,896,2048]{2,1,0:T(8,128)(2,1)} %param.34) | copy-start | bytes 11010052
  128.0 1.6 copy-start.1
  128.0 2.1 copy-start.6
  128.0 4.3 %copy-start.3 = (bf16[2048,64]{0,1:T(8,128)(2,1)S(1)}, bf16[2048,64]{0,1:T(8,128)(2,1)}, u32[]{:S(2)}) copy-start(bf16[2048,64]{0,1:T(8,128)(2,1)} %param.24) | copy-start | bytes 786436
  130.1 35.5 %copy-start.4 = (bf16[2048,64]{0,1:T(8,128)(2,1)S(1)}, bf16[2048,64]{0,1:T(8,128)(2,1)}, u32[]{:S(2)}) copy-start(bf16[2048,64]{0,1:T(8,128)(2,1)} %param.25) | copy-start | bytes 786436
  219.4 67.7 %copy-start.9 = (f32[256,2]{0,1:T(2,128)S(1)}, f32[256,2]{0,1:T(2,128)}, u32[]{:S(2)}) copy-start(f32[256,2]{0,1:T(2,128)} %param.30) | copy-start | bytes 6148
  220.2 9.4 %all-to-all-start = ((bf16[4,128,256]{1,2,0:T(8,128)(2,1)}), bf16[4,128,256]{1,2,0:T(8,128)(2,1)S(1)}, u32[]{:S(2)}, u32[]{:S(2)}) async-start(bf16[4,128,256]{1,2,0:T(8,128)(2,1)} %copy.39), calls=%async_computation | async-start | bytes 524288 | tf_op jit(solution)/shard_map/all_to_all | solution.py:111
  226.5 63.9 %copy-start.7 = (f32[2048]{0:T(1024)S(1)}, f32[2048]{0:T(1024)}, u32[]{:S(2)}) copy-start(f32[2048]{0:T(1024)} %param.27) | copy-start | bytes 24580
  229.6 83.1 %all-to-all-start.2 = ((bf16[32,8,2048]{2,0,1:T(8,128)(2,1)}), bf16[32,8,2048]{2,0,1:T(8,128)(2,1)S(1)}, u32[]{:S(2)}, u32[]{:S(2)}) async-start(bf16[32,8,2048]{2,0,1:T(8,128)(2,1)} %copy.46), calls=%async_computation.3 | async-start | bytes 2097152 | tf_op jit(solution)/shard_map/all_to_all | solution.py:169
  313.3 3.3 %copy-start.8 = (f32[2048]{0:T(1024)S(1)}, f32[2048]{0:T(1024)}, u32[]{:S(2)}) copy-start(f32[2048]{0:T(1024)} %param.35) | copy-start | bytes 24580
Sparse Core Ops, SparseCore 0:
  76.2 33.4 all-gather.4
  128.1 44.5 reduce-scatter.1
where the time goes:
time: 326 us; the launch traced here: 324 us
  blocking collectives  95.8 us (29%)
  starting transfers between devices  61.1 us (19%)
  waiting for transfers between devices  58 us (18%)
  local copies, waits for them, and re-layouts  51.1 us (16%)
  matrix products  29 us (9%)
  between operations  14.4 us (4%)
  other arithmetic  9.24 us (3%)
  loops' own time  5.57 us (2%)
    all_to_all x1, starting transfers between devices, expert_half(): lax.all_to_all(results, 'ep', split_axis=1, concat_axis=1, tiled=True)  57.5 us
    all_gather x1, waiting for transfers between devices, expert_half(): slot_rows = lax.all_gather(arrived[None], 'tp', axis=0, tiled=True)  33.4 us
    all_to_all x1, blocking collectives, expert_half(): lax.all_to_all(outgoing, 'ep', split_axis=1, concat_axis=1, tiled=True)  32.9 us
    all_gather x1, blocking collectives, mixer_half(): key_piece = lax.all_gather(key_rows, 'ep', axis=0, tiled=True)  31.5 us
    all_gather x1, blocking collectives, mixer_half(): value_piece = lax.all_gather(value_rows, 'ep', axis=0, tiled=True)  31.4 us
    scatter x1, local copies, waits for them, and re-layouts, expert_half(): slot_table = jnp.full((quarters, slot_count, experts), row_count, jnp.int...  29.5 us
    all_to_all x1, waiting for transfers between devices, expert_half(): lax.all_to_all(results, 'ep', split_axis=1, concat_axis=1, tiled=True)  21.4 us
    dot_general x1, matrix products, expert_half(): up_part = jnp.dot(flat_rows, up_local, preferred_element_type=jnp.float32)  7.49 us
  transfers between devices with their start and end apart: 4, of which 3 were waited for; matrix products, arithmetic and copies ran while one was open for 9% of the time, Pallas kernels for 0%

commit v1 on v0

v1 whole, which is shorter than its diff:
```python
import functools

import jax
import jax.numpy as jnp
from jax import lax
from jax.experimental import pallas as pl
from jax.experimental.pallas import tpu as pltpu
from jax.sharding import PartitionSpec as P

HD = 64
TOP_K = 2


NEG_FILL = -1e30
NORM_EPS = 1e-06


def norm_rows(values_in, gain_vec):
    widened = values_in.astype(jnp.float32)
    return (
        widened
        * lax.rsqrt(jnp.mean(widened * widened, axis=-1, keepdims=True) + NORM_EPS)
        * gain_vec
    )


def attention_kernel(rows, heads, q_ref, kv_ref, gate_ref, out_ref, max_ref, acc_ref):
    own = lax.axis_index("ep")
    max_ref[...] = jnp.full(max_ref.shape, NEG_FILL, jnp.float32)
    acc_ref[...] = jnp.zeros(acc_ref.shape, jnp.float32)

    def block(index, diagonal):
        first = pl.multiple_of(index * rows, rows)
        kv = kv_ref[pl.ds(first, rows), :]
        keys = kv[:, :HD]
        lane = lax.broadcasted_iota(jnp.int32, kv.shape, 1)
        values = jnp.where(lane < HD, jnp.ones_like(kv), kv)
        gates = gate_ref[:, pl.ds(first, rows)]
        for head in range(heads):
            scores = lax.dot_general(
                q_ref[head], keys, (((1,), (1,)), ((), ())), preferred_element_type=jnp.float32
            )
            scores = scores - gates[head : head + 1, :]
            if diagonal:
                row = lax.broadcasted_iota(jnp.int32, scores.shape, 0)
                column = lax.broadcasted_iota(jnp.int32, scores.shape, 1)
                scores = jnp.where(column <= row, scores, NEG_FILL)
            old_max = max_ref[head][:, :1]
            new_max = jnp.maximum(old_max, jnp.max(scores, axis=1, keepdims=True))
            shifted = jnp.exp(scores - new_max).astype(jnp.bfloat16)
            acc_ref[head] = acc_ref[head] * jnp.exp(old_max - new_max) + jnp.dot(
                shifted, values, preferred_element_type=jnp.float32
            )
            max_ref[head] = jnp.broadcast_to(new_max, max_ref.shape[1:])

    def earlier(index, carry):
        block(index, False)
        return carry

    lax.fori_loop(0, own, earlier, 0)
    block(own, True)
    for head in range(heads):
        total = acc_ref[head]
        out_ref[head] = (total[:, HD:] / total[:, :HD]).astype(out_ref.dtype)


def attend(queries, kv_rows, gate_totals):
    heads, rows, _ = queries.shape
    return pl.pallas_call(
        functools.partial(attention_kernel, rows, heads),
        out_shape=jax.ShapeDtypeStruct(queries.shape, jnp.bfloat16),
        in_specs=[pl.BlockSpec(memory_space=pltpu.VMEM)] * 3,
        out_specs=pl.BlockSpec(memory_space=pltpu.VMEM),
        scratch_shapes=[
            pltpu.VMEM((heads, rows, 2 * HD), jnp.float32),
            pltpu.VMEM((heads, rows, 2 * HD), jnp.float32),
        ],
        cost_estimate=pl.CostEstimate(
            flops=30_000_000_000, bytes_accessed=4_000_000, transcendentals=0
        ),
        compiler_params=pltpu.CompilerParams(vmem_limit_bytes=32 * 1024 * 1024),
    )(queries, kv_rows, gate_totals)


def mixer_half(
    mixer_input, log_forget_total, mixer_gain, w_query, w_key, w_value, w_output, mixer_post_gain
):
    row_count = mixer_input.shape[0]
    head_local = w_query.shape[1] // HD
    normed = norm_rows(mixer_input, mixer_gain).astype(jnp.bfloat16)
    w_kv = jnp.concatenate([w_key, w_value], axis=1)
    kv_rows = jnp.dot(normed, w_kv, preferred_element_type=jnp.float32).astype(jnp.bfloat16)
    kv_all = lax.all_gather(kv_rows, "ep", axis=0, tiled=True)
    queries = jnp.dot(normed, w_query, preferred_element_type=jnp.float32).astype(jnp.bfloat16)
    queries = queries * jnp.bfloat16(HD ** (-0.5))
    queries = jnp.transpose(queries.reshape(row_count, head_local, HD), (1, 0, 2))
    mixed = attend(queries, kv_all, log_forget_total)
    mixed_heads = jnp.transpose(mixed, (1, 0, 2)).reshape(row_count, head_local * HD)
    by_rows = lax.all_to_all(mixed_heads, "tp", split_axis=0, concat_axis=1, tiled=True)
    projected = jnp.dot(by_rows, w_output, preferred_element_type=jnp.float32)
    return norm_rows(projected, mixer_post_gain).astype(jnp.bfloat16)


def expert_half(
    expert_input, expert_ids, route_weight, expert_gain, w_gate, w_up, w_down, expert_post_gain
):
    row_count = expert_input.shape[0]
    quarters = lax.axis_size("tp")
    experts = lax.axis_size("ep")
    quarter_rows = row_count // quarters
    slot_count = 2 * TOP_K * quarter_rows // experts
    first = lax.axis_index("tp") * quarter_rows
    own_input = lax.dynamic_slice_in_dim(expert_input, first, quarter_rows, 0)
    own_weights = lax.dynamic_slice_in_dim(route_weight, first, quarter_rows, 0)
    routed = lax.dynamic_slice_in_dim(expert_ids, first, quarter_rows, 0)
    normed = norm_rows(own_input, expert_gain).astype(jnp.bfloat16)
    matches = routed[:, :, None] == jnp.arange(experts, dtype=jnp.int32)[None, None, :]
    matches = matches.astype(jnp.bfloat16)
    per_token = jnp.sum(matches, axis=1)
    position = jnp.arange(quarter_rows, dtype=jnp.int32)
    lower = (position[None, :] < position[:, None]).astype(jnp.bfloat16)
    before = jnp.dot(lower, per_token, preferred_element_type=jnp.float32)
    ranks = jnp.sum(matches.astype(jnp.float32) * before[:, None, :], axis=2).astype(jnp.int32)
    slots = routed * slot_count + ranks
    total_slots = experts * slot_count
    chosen = slots[:, :, None] == jnp.arange(total_slots, dtype=jnp.int32)[None, None, :]
    chosen = chosen.astype(jnp.bfloat16)
    outgoing = lax.dot_general(
        jnp.sum(chosen, axis=1), normed, (((0,), (0,)), ((), ())),
        preferred_element_type=jnp.float32,
    ).astype(jnp.bfloat16)
    arrived = lax.all_to_all(
        outgoing.reshape(experts, slot_count, -1), "ep", split_axis=0, concat_axis=0, tiled=True
    )
    flat_rows = lax.all_gather(
        arrived.reshape(total_slots, -1), "tp", axis=0, tiled=True
    )
    gate_part = jnp.dot(flat_rows, w_gate[0], preferred_element_type=jnp.float32)
    up_part = jnp.dot(flat_rows, w_up[0], preferred_element_type=jnp.float32)
    hidden = (jax.nn.silu(gate_part) * up_part).astype(jnp.bfloat16)
    product = jnp.dot(hidden, w_down[0], preferred_element_type=jnp.float32).astype(jnp.bfloat16)
    results = lax.psum_scatter(product, "tp", scatter_dimension=0, tiled=True)
    returned = lax.all_to_all(
        results.reshape(experts, slot_count, -1), "ep", split_axis=0, concat_axis=0, tiled=True
    ).reshape(total_slots, -1)
    combined = 0.0
    for k in range(TOP_K):
        picked = jnp.dot(chosen[:, k], returned, preferred_element_type=jnp.float32)
        combined = combined + own_weights[:, k : k + 1] * picked
    return norm_rows(combined, expert_post_gain).astype(jnp.bfloat16)


def per_device(
    mixer_input,
    log_forget_total,
    mixer_gain,
    w_query,
    w_key,
    w_value,
    w_output,
    mixer_post_gain,
    expert_input,
    expert_ids,
    route_weight,
    expert_gain,
    w_gate,
    w_up,
    w_down,
    expert_post_gain,
):
    mixer_out = mixer_half(
        mixer_input,
        log_forget_total,
        mixer_gain,
        w_query,
        w_key,
        w_value,
        w_output,
        mixer_post_gain,
    )
    expert_out = expert_half(
        expert_input, expert_ids, route_weight, expert_gain, w_gate, w_up, w_down, expert_post_gain
    )
    return (mixer_out, expert_out)


def solution(mesh):
    placed = (
        P("ep", None),
        P("tp", None),
        P(),
        P(None, "tp"),
        P(None, "tp"),
        P(None, "tp"),
        P(),
        P(),
        P("ep", None),
        P("ep", None),
        P("ep", None),
        P(),
        P("ep", None, "tp"),
        P("ep", None, "tp"),
        P("ep", "tp", None),
        P(),
    )
    return jax.shard_map(
        per_device,
        mesh=mesh,
        in_specs=placed,
        out_specs=(P(("ep", "tp"), None), P(("ep", "tp"), None)),
        check_vma=False,
    )
```

time: 326 us -> 210 us (0.64)
  blocking collectives: 95.8 us -> 41.5 us
  starting transfers between devices: 61.1 us -> 8.6 us
  local copies, waits for them, and re-layouts: 51.1 us -> 2.84 us
  waiting for transfers between devices: 58 us -> 106 us
  loops' own time: 5.57 us -> 0 us
  other arithmetic: 9.24 us -> 4.35 us
  Pallas kernels: 0 us -> 4.74 us
    all_gather x2 -> x0, blocking collectives: 62.9 us -> none  [the longest x1 31.5 us: mixer_half(): key_piece = lax.all_gather(key_rows, 'ep', axis=0, tiled=True)]
    all_to_all x2 -> x1, starting transfers between devices: 60.9 us -> 8.48 us  [expert_half(): lax.all_to_all(results.reshape(experts, slot_count, -1), 'ep', split_axis...]
    reduce_scatter x1, waiting for transfers between devices: 0.02 us -> 31 us  [expert_half(): results = lax.psum_scatter(product, 'tp', scatter_dimension=0, tiled=True)]
    scatter x1 -> x0, local copies, waits for them, and re-layouts: 29.5 us -> none  [expert_half(): slot_table = jnp.full((quarters, slot_count, experts), row_count, jnp.int...]
    all_gather x1 -> x2, waiting for transfers between devices: 33.4 us -> 53.9 us  [the longest x1 30.6 us: expert_half(): lax.all_gather(arrived.reshape(total_slots, -1), 'tp', axis=0, tiled=True)]
    all_to_all x1 -> x2, blocking collectives: 32.9 us -> 41.5 us  [the longest x1 33 us: expert_half(): lax.all_to_all(outgoing.reshape(experts, slot_count, -1), 'ep', split_axi...]
    another operation x9 -> x0, loops' own time: 5.57 us -> none  [the longest x1 5.43 us: mixer_half(): lax.scan(one_block, running, (key_blocks, value_blocks, jnp.arange(block_...]
    dynamic_slice x11 -> x2, local copies, waits for them, and re-layouts: 6.09 us -> 0.98 us  [the longest x1 0.9 us: expert_half(): routed = lax.dynamic_slice_in_dim(expert_ids, first, quarter_rows, 0)]
  transfers between devices with their start and end apart: 4 -> 4, of which waited for: 3 -> 4; matrix products, arithmetic and copies ran while one was open for 9% -> 13% of each run, Pallas kernels for 0% -> 2%
where the time goes in v1:
time: 210 us; the launch traced here: 209 us
  waiting for transfers between devices  106 us (50%)
  blocking collectives  41.5 us (20%)
  matrix products  26.9 us (13%)
  between operations  14 us (7%)
  starting transfers between devices  8.6 us (4%)
  Pallas kernels  4.74 us (2%)
  other arithmetic  4.35 us (2%)
  local copies, waits for them, and re-layouts  2.84 us (1%)
    all_to_all x1, blocking collectives, expert_half(): lax.all_to_all(outgoing.reshape(experts, slot_count, -1), 'ep', split_axi...  33 us
    reduce_scatter x1, waiting for transfers between devices, expert_half(): results = lax.psum_scatter(product, 'tp', scatter_dimension=0, tiled=True)  31 us
    all_gather x1, waiting for transfers between devices, expert_half(): lax.all_gather(arrived.reshape(total_slots, -1), 'tp', axis=0, tiled=True)  30.6 us
    all_gather x1, waiting for transfers between devices, mixer_half(): kv_all = lax.all_gather(kv_rows, 'ep', axis=0, tiled=True)  23.3 us
    all_to_all x1, waiting for transfers between devices, expert_half(): lax.all_to_all(results.reshape(experts, slot_count, -1), 'ep', split_axis...  21.5 us
    all_to_all x1, blocking collectives, mixer_half(): lax.all_to_all(mixed_heads, 'tp', split_axis=0, concat_axis=1, tiled=True)  8.54 us
    all_to_all x1, starting transfers between devices, expert_half(): lax.all_to_all(results.reshape(experts, slot_count, -1), 'ep', split_axis...  8.48 us
    dot_general x1, matrix products, expert_half(): up_part = jnp.dot(flat_rows, w_up[0], preferred_element_type=jnp.float32)  7.49 us
  transfers between devices with their start and end apart: 4, of which 4 were waited for; matrix products, arithmetic and copies ran while one was open for 13% of the time, Pallas kernels for 2%

profile of v1, /device:TPU:0, one launch (start us, length us, event | category | flops | bytes accessed | tf_op | source)
XLA Modules:
  0.0 209.5 jit_solution(4540736557848949332)
XLA Ops:
  7.2 0.0 copy-start
  7.2 0.0 copy-start.3
  7.2 0.0 copy-start.11
  7.2 0.0 copy-start.10
  7.2 0.0 all-gather.5.cloned.1.call-start
  7.3 0.9 constant_dynamic-slice_fusion
  8.2 0.1 fusion.24
  8.3 0.8 convert_add_fusion
  9.1 0.1 convert_reduce_fusion
  9.2 1.1 fusion.14
  10.3 1.5 convolution_convert_fusion.1
  11.8 33.0 %all_to_all.29 = bf16[8,32,2048]{2,1,0:T(8,128)(2,1)} all-to-all(bf16[8,32,2048]{2,1,0:T(8,128)(2,1)S(1)} %bitcast.50), channel_id=1, replica_groups=mesh['ep'=8,'tp'=4] {'ep'}, dimensions={0} | all-to-all | bytes 2097152 | tf_op jit(solution)/shard_map/all_to_all | solution.py:132
  44.8 0.0 all-gather.5.cloned.1.call-update
  44.8 0.0 all-gather.3.cloned.1.call-start
  44.8 0.5 fusion
  45.3 0.0 copy-done.10
  45.4 2.4 %convolution_convert_fusion.3 = bf16[512,128]{1,0:T(8,128)(2,1)} fusion(bf16[512,2048]{1,0:T(8,128)(2,1)S(1)} %copy-done.3, f32[2048]{0:T(1024)S(1)} %copy-done.11, f32[512]{0:T(512)S(1)} %add_rsqrt_fusion, bf16[2048,64]{0,1:T(8,128)(2,1)S(1)} %copy-done.10, bf16[2048,64]{0,1:T(8,128)(2,1)} %param.20), kind=kOutput, calls=%fused_computation.18 | convolution fusion | flops 273743872 | bytes 2762752 | tf_op jit(solution)/shard_map/dot_general | solution.py:92
  47.7 0.0 all-gather.3.cloned.1.call-update
  47.7 0.0 reduce-scatter.2.cloned.1.call-start
  47.8 30.6 %all-gather.5.cloned.1.call-done = bf16[1024,2048]{1,0:T(8,128)(2,1)} async-done(((bf16[256,2048]{1,0:T(8,128)(2,1)}), bf16[1024,2048]{1,0:T(8,128)(2,1)}) %all-gather.5.cloned.1.call-update) | async-done | bytes 4194320 | tf_op jit(solution)/shard_map/all_gather | solution.py:135
  78.4 7.5 %fusion.4 = f32[1024,896]{1,0:T(8,128)S(1)} fusion(bf16[1024,2048]{1,0:T(8,128)(2,1)} %all-gather.5.cloned.1.call-done, bf16[1,2048,896]{2,1,0:T(8,128)(2,1)} %param.29), kind=kOutput, calls=%fused_computation.7 | convolution fusion | flops 3758096384 | bytes 11534336 | tf_op jit(solution)/shard_map/dot_general | solution.py:139
  85.9 0.0 copy-start.9
  85.9 4.8 %multiply_convert_fusion = bf16[1024,896]{1,0:T(8,128)(2,1)S(1)} fusion(f32[1024,896]{1,0:T(8,128)S(1)} %fusion.4, bf16[1024,2048]{1,0:T(8,128)(2,1)S(1)} %copy-done.7, bf16[1,2048,896]{2,1,0:T(8,128)(2,1)S(1)} %copy-done.8), kind=kOutput, calls=%fused_computation.11 | convolution fusion | flops 3763601408 | bytes 13369344 | tf_op jit(solution)/shard_map/dot_general | solution.py:138
  90.8 6.0 %convolution_convert_fusion = bf16[1024,2048]{1,0:T(8,128)(2,1)} fusion(bf16[1024,896]{1,0:T(8,128)(2,1)S(1)} %multiply_convert_fusion, bf16[1,896,2048]{2,1,0:T(8,128)(2,1)S(1)} %copy-done.9), kind=kOutput, calls=%fused_computation.5 | convolution fusion | flops 3760193536 | bytes 9699328 | tf_op jit(solution)/shard_map/dot_general | solution.py:141
  96.8 0.0 reduce-scatter.2.cloned.1.call-update
  96.8 0.0 copy-start.2
  96.9 0.9 fusion.11
  97.8 0.3 copy.31
  98.1 23.3 %all-gather.3.cloned.1.call-done.kv_ref = bf16[4096,128]{1,0:T(8,128)(2,1)} async-done(((bf16[512,128]{1,0:T(8,128)(2,1)}), bf16[4096,128]{1,0:T(8,128)(2,1)}) %all-gather.3.cloned.1.call-update) | async-done | bytes 1048592 | tf_op jit(solution)/shard_map/all_gather | solution.py:93
  121.4 1.2 copy-done.1
  122.6 4.7 %shard_map.167 = bf16[4,512,64]{2,1,0:T(8,128)(2,1)S(1)} custom-call(bf16[4,512,64]{2,1,0:T(8,128)(2,1)S(1)} %bitcast.45, bf16[4096,128]{1,0:T(8,128)(2,1)S(1)} %copy-done.1, f32[4,4096]{1,0:T(4,128)S(1)} %copy-done.2), custom_call_target="tpu_custom_call" | custom-call | flops 30000001024 | bytes 4000000 | tf_op jit(solution)/shard_map/pallas_call | solution.py:69
  127.4 0.0 copy-start.6
  127.4 0.2 copy.32
  127.6 0.1 all_to_all.20
  127.7 8.5 %all_to_all.30 = bf16[4,128,256]{1,2,0:T(8,128)(2,1)S(1)} all-to-all(bf16[4,128,256]{1,2,0:T(8,128)(2,1)S(1)} %copy.33), channel_id=1, replica_groups=mesh['ep'=8,'tp'=4] {'tp'}, dimensions={0} | all-to-all | bytes 524288 | tf_op jit(solution)/shard_map/all_to_all | solution.py:99
  136.2 31.0 %reduce-scatter.2.cloned.1.call-done = bf16[256,2048]{1,0:T(8,128)(2,1)} async-done(((bf16[1024,2048]{1,0:T(8,128)(2,1)}), bf16[256,2048]{1,0:T(8,128)(2,1)}) %reduce-scatter.2.cloned.1.call-update) | async-done | bytes 1048592 | tf_op jit(solution)/shard_map/reduce_scatter | solution.py:142
  167.3 8.5 %all-to-all-start.2 = ((bf16[8,32,2048]{2,1,0:T(8,128)(2,1)}), bf16[8,32,2048]{2,1,0:T(8,128)(2,1)S(1)}, u32[]{:S(2)}, u32[]{:S(2)}) async-start(bf16[8,32,2048]{2,1,0:T(8,128)(2,1)} %bitcast.52), calls=%async_computation.3 | async-start | bytes 2097152 | tf_op jit(solution)/shard_map/all_to_all | solution.py:143
  175.7 0.0 copy-done.6
  175.7 0.1 constant_dynamic-slice_fusion.1
  175.8 0.1 iota_compare_fusion
  175.9 3.0 %multiply_reduce_fusion = (f32[128]{0:T(128)S(1)}, f32[128,2048]{1,0:T(8,128)S(1)}) fusion(bf16[128,1024]{0,1:T(8,128)(2,1)S(1)} %bitcast.51, bf16[1024,2048]{1,0:T(8,128)(2,1)} %param.22), kind=kOutput, calls=%fused_computation.20 | convolution fusion | flops 537395072 | bytes 5505536 | tf_op jit(solution)/shard_map/dot_general | solution.py:100
  178.9 0.0 copy-start.5
  179.0 0.0 copy-done.4
  179.0 1.0 multiply_convert_fusion.1
  179.9 21.5 %all-to-all-done.2 = bf16[8,32,2048]{2,1,0:T(8,128)(2,1)S(1)} async-done(((bf16[8,32,2048]{2,1,0:T(8,128)(2,1)}), bf16[8,32,2048]{2,1,0:T(8,128)(2,1)S(1)}, u32[]{:S(2)}, u32[]{:S(2)}) %all-to-all-start.2) | async-done | bytes 1048608 | tf_op jit(solution)/shard_map/all_to_all | solution.py:143
  201.4 0.3 convolution_multiply_fusion.1
  201.7 0.4 multiply_reduce_fusion.1
  202.1 0.8 multiply_convert_fusion.2
  (20 shorter events, 0.1 us)
Async XLA Ops:
  7.2 89.7 %copy-start = (bf16[2048,256]{1,0:T(8,128)(2,1)S(1)}, bf16[2048,256]{1,0:T(8,128)(2,1)}, u32[]{:S(2)}) copy-start(bf16[2048,256]{1,0:T(8,128)(2,1)} %param.19) | copy-start | bytes 3145732
  7.2 37.6 %copy-start.3 = (bf16[512,2048]{1,0:T(8,128)(2,1)S(1)}, bf16[512,2048]{1,0:T(8,128)(2,1)}, u32[]{:S(2)}) copy-start(bf16[512,2048]{1,0:T(8,128)(2,1)} %param.16) | copy-start | bytes 6291460
  7.2 38.1 %copy-start.11 = (f32[2048]{0:T(1024)S(1)}, f32[2048]{0:T(1024)}, u32[]{:S(2)}) copy-start(f32[2048]{0:T(1024)} %param.18) | copy-start | bytes 24580
  7.2 38.1 %copy-start.10 = (bf16[2048,64]{0,1:T(8,128)(2,1)S(1)}, bf16[2048,64]{0,1:T(8,128)(2,1)}, u32[]{:S(2)}) copy-start(bf16[2048,64]{0,1:T(8,128)(2,1)} %param.21) | copy-start | bytes 786436
  7.2 71.2 %all-gather.5.cloned.1.call-start = ((), (), s32[]{:S(2)}) async-start(), calls=%async_computation.5 | async-start | bytes 5242880 | tf_op jit(solution)/shard_map/all_gather | solution.py:135
  44.8 76.6 %all-gather.3.cloned.1.call-start = ((), (), s32[]{:S(2)}) async-start(), calls=%async_computation.4 | async-start | bytes 1179648 | tf_op jit(solution)/shard_map/all_gather | solution.py:93
  47.7 119.5 %reduce-scatter.2.cloned.1.call-start = ((), (), s32[]{:S(2)}) async-start(), calls=%async_computation.6 | async-start | bytes 5242880 | tf_op jit(solution)/shard_map/reduce_scatter | solution.py:142
  78.4 7.5 %copy-start.7 = (bf16[1024,2048]{1,0:T(8,128)(2,1)S(1)}, bf16[1024,2048]{1,0:T(8,128)(2,1)}, u32[]{:S(2)}) copy-start(bf16[1024,2048]{1,0:T(8,128)(2,1)} %all-gather.5.cloned.1.call-done) | copy-start | bytes 12582916
  78.4 7.5 %copy-start.8 = (bf16[1,2048,896]{2,1,0:T(8,128)(2,1)S(1)}, bf16[1,2048,896]{2,1,0:T(8,128)(2,1)}, u32[]{:S(2)}) copy-start(bf16[1,2048,896]{2,1,0:T(8,128)(2,1)} %param.28) | copy-start | bytes 11010052
  85.9 4.8 %copy-start.9 = (bf16[1,896,2048]{2,1,0:T(8,128)(2,1)S(1)}, bf16[1,896,2048]{2,1,0:T(8,128)(2,1)}, u32[]{:S(2)}) copy-start(bf16[1,896,2048]{2,1,0:T(8,128)(2,1)} %param.30) | copy-start | bytes 11010052
  96.8 24.6 %copy-start.2 = (f32[4,4096]{1,0:T(4,128)S(1)}, f32[4,4096]{1,0:T(4,128)}, u32[]{:S(2)}) copy-start(f32[4,4096]{1,0:T(4,128)} %gate_ref.1) | copy-start | bytes 196612
  121.4 1.2 copy-start.1
  127.4 48.4 %copy-start.6 = (f32[256,2]{0,1:T(2,128)S(1)}, f32[256,2]{0,1:T(2,128)}, u32[]{:S(2)}) copy-start(f32[256,2]{0,1:T(2,128)} %param.26) | copy-start | bytes 6148
  167.3 11.7 %copy-start.4 = (f32[2048]{0:T(1024)S(1)}, f32[2048]{0:T(1024)}, u32[]{:S(2)}) copy-start(f32[2048]{0:T(1024)} %param.23) | copy-start | bytes 24580
  167.3 34.1 %all-to-all-start.2 = ((bf16[8,32,2048]{2,1,0:T(8,128)(2,1)}), bf16[8,32,2048]{2,1,0:T(8,128)(2,1)S(1)}, u32[]{:S(2)}, u32[]{:S(2)}) async-start(bf16[8,32,2048]{2,1,0:T(8,128)(2,1)} %bitcast.52), calls=%async_computation.3 | async-start | bytes 2097152 | tf_op jit(solution)/shard_map/all_to_all | solution.py:143
  178.9 23.2 %copy-start.5 = (f32[2048]{0:T(1024)S(1)}, f32[2048]{0:T(1024)}, u32[]{:S(2)}) copy-start(f32[2048]{0:T(1024)} %param.31) | copy-start | bytes 24580
Sparse Core Ops, SparseCore 0:
  44.9 33.4 all-gather.4
  81.1 40.2 all-gather.2
  123.9 43.2 reduce-scatter.1

commit v2 on v1

v2 whole, which is shorter than its diff:
```python
import functools

import jax
import jax.numpy as jnp
from jax import lax
from jax.experimental import pallas as pl
from jax.experimental.pallas import tpu as pltpu
from jax.sharding import PartitionSpec as P

HD = 64
TOP_K = 2


NEG_FILL = -1e30
NORM_EPS = 1e-06


def norm_rows(values_in, gain_vec):
    widened = values_in.astype(jnp.float32)
    return (
        widened
        * lax.rsqrt(jnp.mean(widened * widened, axis=-1, keepdims=True) + NORM_EPS)
        * gain_vec
    )


def meet(axis_sizes):
    barrier = pltpu.get_barrier_semaphore()
    for axis, size in axis_sizes:
        place = lax.axis_index(axis)
        for step in range(1, size):
            pl.semaphore_signal(
                barrier,
                inc=1,
                device_id={axis: lax.rem(place + step, size)},
                device_id_type=pl.DeviceIdType.MESH,
            )
    pl.semaphore_wait(barrier, sum(size - 1 for _, size in axis_sizes))


def push(source, target, sems, index, axis, place):
    return pltpu.make_async_remote_copy(
        src_ref=source,
        dst_ref=target,
        send_sem=sems.at[0, index],
        recv_sem=sems.at[1, index],
        device_id={axis: place},
        device_id_type=pl.DeviceIdType.MESH,
    )


def inward_kernel(
    n_ep, rows, heads, q_ref, kv_ref, gate_ref, out_rows, mixed_ref, slots_ref,
    kv_all, max_ref, acc_ref, kv_sem, ep_sem, x_sem, c_sem, d_sem,
):
    own = lax.axis_index("ep")
    quarter = lax.axis_index("tp")
    across = lax.rem(quarter + 2, 4)
    beside = quarter + 1 - 2 * lax.rem(quarter, 2)
    max_ref[...] = jnp.full(max_ref.shape, NEG_FILL, jnp.float32)
    acc_ref[...] = jnp.zeros(acc_ref.shape, jnp.float32)
    meet((("ep", n_ep), ("tp", 4)))

    def block(kv, index, diagonal):
        first = pl.multiple_of(index * rows, rows)
        keys = kv[:, :HD]
        lane = lax.broadcasted_iota(jnp.int32, kv.shape, 1)
        values = jnp.where(lane < HD, jnp.ones_like(kv), kv)
        gates = gate_ref[:, pl.ds(first, rows)]
        for head in range(heads):
            scores = lax.dot_general(
                q_ref[head], keys, (((1,), (1,)), ((), ())), preferred_element_type=jnp.float32
            )
            scores = scores - gates[head : head + 1, :]
            if diagonal:
                row = lax.broadcasted_iota(jnp.int32, scores.shape, 0)
                column = lax.broadcasted_iota(jnp.int32, scores.shape, 1)
                scores = jnp.where(column <= row, scores, NEG_FILL)
            old_max = max_ref[head][:, :1]
            new_max = jnp.maximum(old_max, jnp.max(scores, axis=1, keepdims=True))
            shifted = jnp.exp(scores - new_max).astype(jnp.bfloat16)
            acc_ref[head] = acc_ref[head] * jnp.exp(old_max - new_max) + jnp.dot(
                shifted, values, preferred_element_type=jnp.float32
            )
            max_ref[head] = jnp.broadcast_to(new_max, max_ref.shape[1:])

    def kv_copy(source, place):
        return push(kv_ref, kv_all.at[source], kv_sem, source, "ep", place)

    def ep_copy(source, place):
        return pltpu.make_async_remote_copy(
            src_ref=out_rows.at[place],
            dst_ref=slots_ref.at[quarter, source],
            send_sem=ep_sem.at[0, place],
            recv_sem=ep_sem.at[1, source],
            device_id={"ep": place},
            device_id_type=pl.DeviceIdType.MESH,
        )

    def kv_send(place):
        return pltpu.make_async_remote_copy(
            src_ref=kv_ref,
            dst_ref=kv_all.at[own],
            send_sem=kv_sem.at[0, place],
            recv_sem=kv_sem.at[1, own],
            device_id={"ep": place},
            device_id_type=pl.DeviceIdType.MESH,
        )

    def to_across(source, held):
        return push(held, slots_ref.at[quarter, source], x_sem, source, "tp", across)

    def to_beside(source, held):
        return push(held, slots_ref.at[quarter, source], c_sem, source, "tp", beside)

    def second(source):
        held = slots_ref.at[across, source]
        return push(held, slots_ref.at[across, source], d_sem, source, "tp", beside)

    def send(step, carry):
        @pl.when(own + step < n_ep)
        def _():
            kv_send(own + step).start()

        ep_copy(own, lax.rem(own + step, n_ep)).start()
        return carry

    lax.fori_loop(1, n_ep, send, 0)
    to_across(own, out_rows.at[own]).start()
    to_beside(own, out_rows.at[own]).start()
    slots_ref[quarter, own] = out_rows[own]
    block(kv_ref[...], own, True)

    def work(step, carry):
        @pl.when(step <= own)
        def _():
            kv_copy(own - step, own).wait_recv()
            block(kv_all[own - step], own - step, False)

        source = lax.rem(own - step + n_ep, n_ep)
        ep_copy(source, source).wait_recv()
        held = slots_ref.at[quarter, source]
        to_across(source, held).start()
        to_beside(source, held).start()
        earlier = lax.rem(own - step + 1 + n_ep, n_ep)
        to_across(earlier, slots_ref.at[across, earlier]).wait_recv()
        second(earlier).start()
        return carry

    lax.fori_loop(1, n_ep, work, 0)
    last = lax.rem(own + 1, n_ep)
    to_across(last, slots_ref.at[across, last]).wait_recv()
    second(last).start()
    for head in range(heads):
        total = acc_ref[head]
        mixed_ref[head] = (total[:, HD:] / total[:, :HD]).astype(mixed_ref.dtype)

    def drain(step, carry):
        place = lax.rem(own + step, n_ep)

        @pl.when((step > 0) & (own + step < n_ep))
        def _():
            kv_send(own + step).wait_send()

        @pl.when(step > 0)
        def _():
            ep_copy(own, place).wait_send()

        to_across(place, out_rows.at[own]).wait_send()
        to_beside(place, out_rows.at[own]).wait()
        second(place).wait()
        return carry

    lax.fori_loop(0, n_ep, drain, 0)


def inward(queries, kv_rows, gate_totals, outgoing):
    heads, rows, _ = queries.shape
    n_ep, slot_count, width = outgoing.shape
    pair = pltpu.SemaphoreType.DMA((2, n_ep))
    return pl.pallas_call(
        functools.partial(inward_kernel, n_ep, rows, heads),
        out_shape=(
            jax.ShapeDtypeStruct(queries.shape, jnp.bfloat16),
            jax.ShapeDtypeStruct((4, n_ep, slot_count, width), jnp.bfloat16),
        ),
        in_specs=[pl.BlockSpec(memory_space=pltpu.VMEM)] * 4,
        out_specs=[pl.BlockSpec(memory_space=pltpu.VMEM)] * 2,
        scratch_shapes=[
            pltpu.VMEM((n_ep, rows, 2 * HD), jnp.bfloat16),
            pltpu.VMEM((heads, rows, 2 * HD), jnp.float32),
            pltpu.VMEM((heads, rows, 2 * HD), jnp.float32),
            pair, pair, pair, pair, pair,
        ],
        compiler_params=pltpu.CompilerParams(
            collective_id=0, has_side_effects=True, vmem_limit_bytes=40 * 1024 * 1024
        ),
    )(queries, kv_rows, gate_totals, outgoing)


def outward_kernel(
    n_ep, product_ref, mixed_ref, heads_ref, result_ref,
    arrived, summed, crossed, final, h_sem, p_sem, r_sem, x_sem, ep_sem,
):
    own = lax.axis_index("ep")
    quarter = lax.axis_index("tp")
    across = lax.rem(quarter + 2, 4)
    beside = quarter + 1 - 2 * lax.rem(quarter, 2)
    diagonal = lax.rem(beside + 2, 4)
    meet((("ep", n_ep), ("tp", 4)))

    def heads_copy(step):
        place = lax.rem(quarter + step, 4)
        return pltpu.make_async_remote_copy(
            src_ref=mixed_ref.at[place],
            dst_ref=heads_ref.at[quarter],
            send_sem=h_sem.at[0, step],
            recv_sem=h_sem.at[1, step],
            device_id={"tp": place},
            device_id_type=pl.DeviceIdType.MESH,
        )

    def near(j):
        return push(product_ref.at[beside, j], arrived.at[0, j], p_sem, j, "tp", beside)

    def far(j):
        return push(product_ref.at[diagonal, j], arrived.at[1, j], r_sem, j, "tp", beside)

    def cross(j):
        return push(summed.at[j], crossed.at[j], x_sem, j, "tp", across)

    def home(j, source):
        return pltpu.make_async_remote_copy(
            src_ref=final.at[j],
            dst_ref=result_ref.at[source],
            send_sem=ep_sem.at[0, j],
            recv_sem=ep_sem.at[1, source],
            device_id={"ep": j},
            device_id_type=pl.DeviceIdType.MESH,
        )

    def begin(step, carry):
        j = lax.rem(own + step, n_ep)
        far(j).start()
        near(j).start()
        return carry

    lax.fori_loop(1, n_ep + 1, begin, 0)
    for step in range(1, 4):
        heads_copy(step).start()
    heads_ref[quarter] = mixed_ref[quarter]

    def pair_sum(step, carry):
        j = lax.rem(own + step, n_ep)
        far(j).wait_recv()
        total = product_ref[across, j].astype(jnp.float32) + arrived[1, j].astype(jnp.float32)
        summed[j] = total.astype(jnp.bfloat16)
        cross(j).start()
        return carry

    lax.fori_loop(1, n_ep + 1, pair_sum, 0)

    def finish(j):
        near(j).wait_recv()
        cross(j).wait_recv()
        total = product_ref[quarter, j].astype(jnp.float32) + arrived[0, j].astype(jnp.float32)
        return (total + crossed[j].astype(jnp.float32)).astype(jnp.bfloat16)

    def full_sum(step, carry):
        j = lax.rem(own + step, n_ep)
        final[j] = finish(j)
        home(j, own).start()
        return carry

    lax.fori_loop(1, n_ep, full_sum, 0)
    result_ref[own] = finish(own)
    for step in range(1, 4):
        heads_copy(step).wait()

    def drain(step, carry):
        j = lax.rem(own + step, n_ep)
        near(j).wait_send()
        far(j).wait_send()
        cross(j).wait_send()

        @pl.when(step < n_ep)
        def _():
            home(j, own).wait_send()
            home(j, j).wait_recv()

        return carry

    lax.fori_loop(1, n_ep + 1, drain, 0)


def outward(product, mixed):
    _, n_ep, slot_count, width = product.shape
    pair = pltpu.SemaphoreType.DMA((2, n_ep))
    chunk = (n_ep, slot_count, width)
    return pl.pallas_call(
        functools.partial(outward_kernel, n_ep),
        out_shape=(
            jax.ShapeDtypeStruct(mixed.shape, jnp.bfloat16),
            jax.ShapeDtypeStruct(chunk, jnp.bfloat16),
        ),
        in_specs=[pl.BlockSpec(memory_space=pltpu.VMEM)] * 2,
        out_specs=[pl.BlockSpec(memory_space=pltpu.VMEM)] * 2,
        scratch_shapes=[
            pltpu.VMEM((2,) + chunk, jnp.bfloat16),
            pltpu.VMEM(chunk, jnp.bfloat16),
            pltpu.VMEM(chunk, jnp.bfloat16),
            pltpu.VMEM(chunk, jnp.bfloat16),
            pltpu.SemaphoreType.DMA((2, 4)),
            pair, pair, pair, pair,
        ],
        compiler_params=pltpu.CompilerParams(
            collective_id=1, has_side_effects=True, vmem_limit_bytes=40 * 1024 * 1024
        ),
    )(product, mixed)


def attention_inputs(mixer_input, mixer_gain, w_query, w_key, w_value):
    row_count = mixer_input.shape[0]
    head_local = w_query.shape[1] // HD
    normed = norm_rows(mixer_input, mixer_gain).astype(jnp.bfloat16)
    w_kv = jnp.concatenate([w_key, w_value], axis=1)
    kv_rows = jnp.dot(normed, w_kv, preferred_element_type=jnp.float32).astype(jnp.bfloat16)
    queries = jnp.dot(normed, w_query, preferred_element_type=jnp.float32).astype(jnp.bfloat16)
    queries = queries * jnp.bfloat16(HD ** (-0.5))
    queries = jnp.transpose(queries.reshape(row_count, head_local, HD), (1, 0, 2))
    return queries, kv_rows


def routed_rows(expert_input, expert_ids, route_weight, expert_gain):
    row_count = expert_input.shape[0]
    quarters = lax.axis_size("tp")
    experts = lax.axis_size("ep")
    quarter_rows = row_count // quarters
    slot_count = 2 * TOP_K * quarter_rows // experts
    first = lax.axis_index("tp") * quarter_rows
    own_input = lax.dynamic_slice_in_dim(expert_input, first, quarter_rows, 0)
    own_weights = lax.dynamic_slice_in_dim(route_weight, first, quarter_rows, 0)
    routed = lax.dynamic_slice_in_dim(expert_ids, first, quarter_rows, 0)
    normed = norm_rows(own_input, expert_gain).astype(jnp.bfloat16)
    matches = routed[:, :, None] == jnp.arange(experts, dtype=jnp.int32)[None, None, :]
    matches = matches.astype(jnp.bfloat16)
    per_token = jnp.sum(matches, axis=1)
    position = jnp.arange(quarter_rows, dtype=jnp.int32)
    lower = (position[None, :] < position[:, None]).astype(jnp.bfloat16)
    before = jnp.dot(lower, per_token, preferred_element_type=jnp.float32)
    ranks = jnp.sum(matches.astype(jnp.float32) * before[:, None, :], axis=2).astype(jnp.int32)
    slots = routed * slot_count + ranks
    total_slots = experts * slot_count
    chosen = slots[:, :, None] == jnp.arange(total_slots, dtype=jnp.int32)[None, None, :]
    chosen = chosen.astype(jnp.bfloat16)
    outgoing = lax.dot_general(
        jnp.sum(chosen, axis=1), normed, (((0,), (0,)), ((), ())),
        preferred_element_type=jnp.float32,
    ).astype(jnp.bfloat16)
    return outgoing.reshape(experts, slot_count, -1), chosen, own_weights


def per_device(
    mixer_input,
    log_forget_total,
    mixer_gain,
    w_query,
    w_key,
    w_value,
    w_output,
    mixer_post_gain,
    expert_input,
    expert_ids,
    route_weight,
    expert_gain,
    w_gate,
    w_up,
    w_down,
    expert_post_gain,
):
    queries, kv_rows = attention_inputs(mixer_input, mixer_gain, w_query, w_key, w_value)
    outgoing, chosen, own_weights = routed_rows(
        expert_input, expert_ids, route_weight, expert_gain
    )
    mixed, slot_rows = inward(queries, kv_rows, log_forget_total, outgoing)
    flat_rows = slot_rows.reshape(-1, slot_rows.shape[-1])
    gate_part = jnp.dot(flat_rows, w_gate[0], preferred_element_type=jnp.float32)
    up_part = jnp.dot(flat_rows, w_up[0], preferred_element_type=jnp.float32)
    hidden = (jax.nn.silu(gate_part) * up_part).astype(jnp.bfloat16)
    product = jnp.dot(hidden, w_down[0], preferred_element_type=jnp.float32).astype(jnp.bfloat16)
    quarters = slot_rows.shape[0]
    heads, rows, _ = mixed.shape
    mixed_heads = jnp.transpose(mixed, (1, 0, 2)).reshape(quarters, rows // quarters, heads * HD)
    head_rows, returned = outward(product.reshape(slot_rows.shape), mixed_heads)
    by_rows = jnp.transpose(head_rows, (1, 0, 2)).reshape(rows // quarters, -1)
    projected = jnp.dot(by_rows, w_output, preferred_element_type=jnp.float32)
    mixer_out = norm_rows(projected, mixer_post_gain).astype(jnp.bfloat16)
    returned = returned.reshape(-1, returned.shape[-1])
    combined = 0.0
    for k in range(TOP_K):
        picked = jnp.dot(chosen[:, k], returned, preferred_element_type=jnp.float32)
        combined = combined + own_weights[:, k : k + 1] * picked
    expert_out = norm_rows(combined, expert_post_gain).astype(jnp.bfloat16)
    return (mixer_out, expert_out)


def solution(mesh):
    placed = (
        P("ep", None),
        P("tp", None),
        P(),
        P(None, "tp"),
        P(None, "tp"),
        P(None, "tp"),
        P(),
        P(),
        P("ep", None),
        P("ep", None),
        P("ep", None),
        P(),
        P("ep", None, "tp"),
        P("ep", None, "tp"),
        P("ep", "tp", None),
        P(),
    )
    return jax.shard_map(
        per_device,
        mesh=mesh,
        in_specs=placed,
        out_specs=(P(("ep", "tp"), None), P(("ep", "tp"), None)),
        check_vma=False,
    )
```

time: 210 us -> 143 us (0.68)
  waiting for transfers between devices: 106 us -> 0 us
  Pallas kernels: 4.74 us -> 106 us
  blocking collectives: 41.5 us -> 0 us
  between operations: 14 us -> 0.93 us
  starting transfers between devices: 8.6 us -> 0 us
  matrix products: 26.9 us -> 23.7 us
  local copies, waits for them, and re-layouts: 2.84 us -> 5.39 us
    pallas_call x1 -> x2, Pallas kernels: 4.74 us -> 106 us  [the longest x1 64.3 us: outward(): pl.pallas_call(functools.partial(outward_kernel, n_ep), out_shape=(jax.Sh...]
    all_gather x2 -> x0, waiting for transfers between devices: 53.9 us -> none  [the longest x1 30.6 us: expert_half(): lax.all_gather(arrived.reshape(total_slots, -1), 'tp', axis=0, tiled=True)]
    all_to_all x2 -> x0, blocking collectives: 41.5 us -> none  [the longest x1 33 us: expert_half(): lax.all_to_all(outgoing.reshape(experts, slot_count, -1), 'ep', split_axi...]
    reduce_scatter x1 -> x0, waiting for transfers between devices: 31 us -> none  [expert_half(): results = lax.psum_scatter(product, 'tp', scatter_dimension=0, tiled=True)]
    all_to_all x1 -> x0, waiting for transfers between devices: 21.5 us -> none  [expert_half(): lax.all_to_all(results.reshape(experts, slot_count, -1), 'ep', split_axis...]
    all_to_all x1 -> x0, starting transfers between devices: 8.48 us -> none  [expert_half(): lax.all_to_all(results.reshape(experts, slot_count, -1), 'ep', split_axis...]
    dot_general x10, matrix products: 26.9 us -> 23.7 us  [the longest x1 7.5 us: per_device(): up_part = jnp.dot(flat_rows, w_up[0], preferred_element_type=jnp.float32)]
  transfers between devices with their start and end apart: 4 -> 0, of which waited for: 4 -> 0; matrix products, arithmetic and copies ran while one was open for 13% -> 0% of each run, Pallas kernels for 2% -> 0%
where the time goes in v2:
time: 143 us; the launch traced here: 142 us
  Pallas kernels  106 us (74%)
  matrix products  23.7 us (17%)
  other arithmetic  6.18 us (4%)
  local copies, waits for them, and re-layouts  5.39 us (4%)
    pallas_call x1, Pallas kernels, outward(): pl.pallas_call(functools.partial(outward_kernel, n_ep), out_shape=(jax.Sh...  64.3 us
    pallas_call x1, Pallas kernels, inward(): pl.pallas_call(functools.partial(inward_kernel, n_ep, rows, heads), out_s...  41.9 us
    dot_general x1, matrix products, per_device(): up_part = jnp.dot(flat_rows, w_up[0], preferred_element_type=jnp.float32)  7.5 us
    dot_general x1, matrix products, per_device(): jnp.dot(hidden, w_down[0], preferred_element_type=jnp.float32)  4.93 us
    dot_general x1, matrix products, per_device(): jnp.dot(flat_rows, w_gate[0], preferred_element_type=jnp.float32)  4.75 us
    reduce_sum x2, other arithmetic, norm_rows(): jnp.mean(widened * widened, axis=-1, keepdims=True) + NORM_EPS  3.41 us

profile of v2, /device:TPU:0, one launch (start us, length us, event | category | flops | bytes accessed | tf_op | source)
XLA Modules:
  0.0 142.3 jit_solution(17316473699311623145)
XLA Ops:
  0.6 0.0 copy-start
  0.6 1.2 fusion.14
  1.9 0.8 constant_dynamic-slice_fusion.1
  2.6 0.7 constant_dynamic-slice_fusion
  3.4 0.1 fusion.24
  3.5 0.8 convert_add_fusion
  4.3 0.0 copy-start.5
  4.3 2.2 %fusion = f32[512]{0:T(512)S(1)} fusion(bf16[512,2048]{1,0:T(8,128)(2,1)} %param.16), kind=kLoop, calls=%fused_computation.2 | loop fusion | flops 3145216 | bytes 2099200 | tf_op jit(solution)/shard_map/reduce_sum | solution.py:22
  6.5 0.1 iota_compare_fusion
  6.6 0.1 convert_reduce_fusion
  6.7 2.4 %convolution_convert_fusion.3.kv_ref = bf16[512,128]{1,0:T(8,128)(2,1)S(1)} fusion(bf16[512,2048]{1,0:T(8,128)(2,1)} %param.16, f32[2048]{0:T(1024)} %param.18, f32[512]{0:T(512)S(1)} %add_rsqrt_fusion, bf16[2048,64]{0,1:T(8,128)(2,1)} %param.21, bf16[2048,64]{0,1:T(8,128)(2,1)} %param.20), kind=kOutput, calls=%fused_computation.18 | convolution fusion | flops 273743872 | bytes 2762752 | tf_op jit(solution)/shard_map/dot_general | solution.py:327
  9.2 0.0 copy-done
  9.2 0.0 copy-done.5
  9.2 0.0 copy-done.11
  9.2 0.0 copy-start.6
  9.2 0.0 copy-start.1
  9.2 1.0 fusion.11
  10.2 0.3 copy.28
  10.5 0.0 copy-done.6
  10.5 1.4 %convolution_convert_fusion.1 = bf16[256,2048]{1,0:T(8,128)(2,1)S(1)} fusion(bf16[64,256]{1,0:T(8,128)(2,1)S(1)} %convert_reduce_fusion, f32[2048]{0:T(1024)S(1)} %copy-done.6, f32[64]{0:T(128)S(1)} %add_rsqrt_fusion.3, bf16[256,2048]{1,0:T(8,128)(2,1)} %param.24, s32[]{:T(128)S(6)} %select_n.2), kind=kOutput, calls=%fused_computation.12 | convolution fusion | flops 68157440 | bytes 1351940 | tf_op jit(solution)/shard_map/dot_general | solution.py:356
  11.9 0.0 copy-done.1
  11.9 41.9 %shard_map.167 = (bf16[4,512,64]{2,1,0:T(8,128)(2,1)S(1)}, bf16[4,8,32,2048]{3,2,1,0:T(8,128)(2,1)S(1)}) custom-call(bf16[4,512,64]{2,1,0:T(8,128)(2,1)S(1)} %bitcast.46, bf16[512,128]{1,0:T(8,128)(2,1)S(1)} %convolution_convert_fusion.3.kv_ref, f32[4,4096]{1,0:T(4,128)S(1)} %copy-done.1, bf16[8,32,2048]{2,1,0:T(8,128)(2,1)S(1)} %bitcast.42), custom_call_target="tpu_custom_call" | custom-call | tf_op jit(solution)/shard_map/pallas_call | solution.py:181
  53.8 0.0 copy-start.2
  53.8 1.9 %copy-done.2 = bf16[4,8,32,2048]{3,2,1,0:T(8,128)(2,1)} copy-done((bf16[4,8,32,2048]{3,2,1,0:T(8,128)(2,1)}, bf16[4,8,32,2048]{3,2,1,0:T(8,128)(2,1)S(1)}, u32[]{:S(2)}) %copy-start.2) | copy-done | bytes 4194328
  55.8 0.4 copy.32
  56.2 0.3 reshape.71.mixed_ref
  56.5 0.0 copy-start.3
  56.5 0.0 copy-start.9
  56.5 7.5 %fusion.4 = f32[1024,896]{1,0:T(8,128)S(1)} fusion(bf16[1024,2048]{1,0:T(8,128)(2,1)} %bitcast.49, bf16[1,2048,896]{2,1,0:T(8,128)(2,1)} %param.29), kind=kOutput, calls=%fused_computation.7 | convolution fusion | flops 3758096384 | bytes 11534336 | tf_op jit(solution)/shard_map/dot_general | solution.py:388
  64.0 0.0 copy-done.3
  64.1 0.0 copy-done.9
  64.1 0.0 copy-start.10
  64.1 4.7 %multiply_convert_fusion = bf16[1024,896]{1,0:T(8,128)(2,1)S(1)} fusion(f32[1024,896]{1,0:T(8,128)S(1)} %fusion.4, bf16[1024,2048]{1,0:T(8,128)(2,1)S(1)} %bitcast.50, bf16[1,2048,896]{2,1,0:T(8,128)(2,1)S(1)} %copy-done.9), kind=kOutput, calls=%fused_computation.11 | convolution fusion | flops 3763601408 | bytes 13369344 | tf_op jit(solution)/shard_map/dot_general | solution.py:387
  68.8 0.0 copy-done.10
  68.8 4.9 %convolution_convert_fusion = bf16[1024,2048]{1,0:T(8,128)(2,1)S(1)} fusion(bf16[1024,896]{1,0:T(8,128)(2,1)S(1)} %multiply_convert_fusion, bf16[1,896,2048]{2,1,0:T(8,128)(2,1)S(1)} %copy-done.10), kind=kOutput, calls=%fused_computation.5 | convolution fusion | flops 3760193536 | bytes 9699328 | tf_op jit(solution)/shard_map/dot_general | solution.py:390
  73.8 0.0 copy-start.7
  73.8 64.3 %shard_map.168 = (bf16[4,128,256]{2,1,0:T(8,128)(2,1)S(1)}, bf16[8,32,2048]{2,1,0:T(8,128)(2,1)S(1)}) custom-call(bf16[4,8,32,2048]{3,2,1,0:T(8,128)(2,1)S(1)} %bitcast.43, bf16[4,128,256]{2,1,0:T(8,128)(2,1)S(1)} %reshape.71.mixed_ref), custom_call_target="tpu_custom_call" | custom-call | tf_op jit(solution)/shard_map/pallas_call | solution.py:300
  138.1 0.2 copy.31
  138.2 0.0 copy-start.4
  138.3 0.3 convolution_multiply_fusion.1
  138.6 0.4 multiply_reduce_fusion.1
  139.0 0.0 copy-start.8
  139.0 0.0 copy-done.7
  139.0 0.8 multiply_convert_fusion.2
  139.8 0.7 copy-done.4
  140.5 0.8 multiply_reduce_fusion
  141.4 0.0 copy-done.8
  141.4 1.0 multiply_convert_fusion.1
  (8 shorter events, 0.1 us)
Async XLA Ops:
  0.6 8.5 %copy-start = (bf16[2048,256]{1,0:T(8,128)(2,1)S(1)}, bf16[2048,256]{1,0:T(8,128)(2,1)}, u32[]{:S(2)}) copy-start(bf16[2048,256]{1,0:T(8,128)(2,1)} %param.19) | copy-start | bytes 3145732
  4.3 4.9 %copy-start.5 = (bf16[512,2048]{1,0:T(8,128)(2,1)S(1)}, bf16[512,2048]{1,0:T(8,128)(2,1)}, u32[]{:S(2)}) copy-start(bf16[512,2048]{1,0:T(8,128)(2,1)} %param.16) | copy-start | bytes 6291460
  4.3 4.9 %copy-start.11 = (f32[2048]{0:T(1024)S(1)}, f32[2048]{0:T(1024)}, u32[]{:S(2)}) copy-start(f32[2048]{0:T(1024)} %param.18) | copy-start | bytes 24580
  9.2 1.3 copy-start.6
  9.2 2.7 %copy-start.1 = (f32[4,4096]{1,0:T(4,128)S(1)}, f32[4,4096]{1,0:T(4,128)}, u32[]{:S(2)}) copy-start(f32[4,4096]{1,0:T(4,128)} %gate_ref.1) | copy-start | bytes 196612
  53.8 1.9 %copy-start.2 = (bf16[4,8,32,2048]{3,2,1,0:T(8,128)(2,1)}, bf16[4,8,32,2048]{3,2,1,0:T(8,128)(2,1)S(1)}, u32[]{:S(2)}) copy-start(bf16[4,8,32,2048]{3,2,1,0:T(8,128)(2,1)S(1)} %get-tuple-element.6) | copy-start | bytes 12582916
  56.5 7.5 %copy-start.3 = (bf16[4,8,32,2048]{3,2,1,0:T(8,128)(2,1)S(1)}, bf16[4,8,32,2048]{3,2,1,0:T(8,128)(2,1)}, u32[]{:S(2)}) copy-start(bf16[4,8,32,2048]{3,2,1,0:T(8,128)(2,1)} %copy-done.2) | copy-start | bytes 12582916
  56.5 7.5 %copy-start.9 = (bf16[1,2048,896]{2,1,0:T(8,128)(2,1)S(1)}, bf16[1,2048,896]{2,1,0:T(8,128)(2,1)}, u32[]{:S(2)}) copy-start(bf16[1,2048,896]{2,1,0:T(8,128)(2,1)} %param.28) | copy-start | bytes 11010052
  64.1 4.8 %copy-start.10 = (bf16[1,896,2048]{2,1,0:T(8,128)(2,1)S(1)}, bf16[1,896,2048]{2,1,0:T(8,128)(2,1)}, u32[]{:S(2)}) copy-start(bf16[1,896,2048]{2,1,0:T(8,128)(2,1)} %param.30) | copy-start | bytes 11010052
  73.8 65.2 %copy-start.7 = (f32[2048]{0:T(1024)S(1)}, f32[2048]{0:T(1024)}, u32[]{:S(2)}) copy-start(f32[2048]{0:T(1024)} %param.31) | copy-start | bytes 24580
  138.2 2.3 %copy-start.4 = (bf16[1024,2048]{1,0:T(8,128)(2,1)S(1)}, bf16[1024,2048]{1,0:T(8,128)(2,1)}, u32[]{:S(2)}) copy-start(bf16[1024,2048]{1,0:T(8,128)(2,1)} %param.22) | copy-start | bytes 12582916
  139.0 2.4 %copy-start.8 = (f32[2048]{0:T(1024)S(1)}, f32[2048]{0:T(1024)}, u32[]{:S(2)}) copy-start(f32[2048]{0:T(1024)} %param.23) | copy-start | bytes 24580
